TPU v7x, 32 devices: a whole 2x2x4 slice. The times are simulated.
32 devices in a mesh: sp: 16 (over z, y, core), dp: 2 (over x).
Axes of the slice: x: 2, y: 2, z: 4, core: 2. Of those that a mesh axis runs over, the one named last changes fastest.
Arguments:
- tokens: bfloat16 [2, 2048, 1024], P('dp', 'sp'), may hold values from -6 to 6
- proj_gate: bfloat16 [1024, 1024], P(('sp', 'dp')), may hold values from -0.1875 to 0.1875
- proj_value: bfloat16 [1024, 1024], P(('sp', 'dp')), may hold values from -0.1875 to 0.1875
- norm_gain: float32 [1024], replicated, may hold values from 0.1 to 1.9
- mix_weight: bfloat16 [4, 1024, 1024], P(None, 'dp'), may hold values from -0.1875 to 0.1875
- mix_bias: float32 [4, 1024], replicated, may hold values from 0.1 to 1.9
- proj_out: bfloat16 [1024, 1024], P(('sp', 'dp')), may hold values from -0.1875 to 0.1875
Outputs:
- mixed: bfloat16 [2, 2048, 1024], P('dp', 'sp')
All inputs are finite; a program needn't handle non-finite values.
Results may differ from a plain program's by a relative error of at most 0.015.
Values may be sent and summed in bfloat16 or wider, within the bound.
A program may use at most 64 MiB of HBM per device.

v0:
```python
import jax
import jax.numpy as jnp
from jax import lax
from jax.sharding import PartitionSpec as P

HEAD_DIM = 256
SPAN = 64


def folded(section, axis, dim, lap, start):
    def gathered(part):
        return lax.all_gather(part, axis, axis=dim, tiled=True)

    return lap(start, jax.tree.map(gathered, section), jnp.int32(0))


def add_rows(total, left, piece, start):
    columns = lax.dynamic_slice_in_dim(left, start, piece.shape[0], 1)
    return total + jnp.dot(columns, piece, preferred_element_type=jnp.float32)


def body(tokens, proj_gate, proj_value, norm_gain, mix_weight, mix_bias, proj_out):
    tok_rows = tokens.shape[1]
    model_width = tokens.shape[2]
    flat = tokens.reshape(tok_rows, model_width)
    width = norm_gain.shape[0]
    groups = lax.axis_size("sp")
    group = width // groups
    empty = jnp.zeros((tok_rows, width), jnp.float32)

    def add_one(total, piece, start):
        return add_rows(total, flat, piece, start)

    u_sum = folded(proj_gate, ("sp", "dp"), 0, add_one, empty)
    v_sum = folded(proj_value, ("sp", "dp"), 0, add_one, empty)
    u_part = u_sum.astype(jnp.bfloat16)
    v_float = v_sum.astype(jnp.bfloat16).astype(jnp.float32)
    centre = jnp.mean(v_float, axis=-1, keepdims=True)
    spread = jnp.mean(jnp.square(v_float - centre), axis=-1, keepdims=True)
    normed = ((v_float - centre) * lax.rsqrt(spread + 1e-05) * norm_gain).astype(jnp.bfloat16)
    head = lax.axis_index("sp") * group // HEAD_DIM
    own_rows = lax.dynamic_index_in_dim(mix_weight, head, 0, keepdims=False)
    head_rows = lax.all_gather(own_rows, "dp", axis=0, tiled=True)
    block = head_rows.shape[1]
    index = jnp.arange(block, dtype=jnp.int32)
    allowed = index[None, :] // SPAN <= index[:, None] // SPAN
    masked = jnp.where(allowed, head_rows, jnp.zeros_like(head_rows))
    bias_row = lax.dynamic_index_in_dim(mix_bias, head, 0, keepdims=False)

    def spatial_mix(sequence):
        channels = sequence.shape[1]
        blocks = sequence.reshape(-1, block, channels)
        result = jnp.einsum("ij,njc->nic", masked, blocks, preferred_element_type=jnp.float32)
        result = result + bias_row[None, :, None]
        return result.astype(jnp.bfloat16).reshape(-1, channels)

    sequence = lax.all_to_all(normed, "sp", split_axis=1, concat_axis=0, tiled=True)
    spatial = lax.all_to_all(spatial_mix(sequence), "sp", split_axis=0, concat_axis=1, tiled=True)
    gated = (u_part.astype(jnp.float32) * spatial.astype(jnp.float32)).astype(jnp.bfloat16)

    def add_out(total, piece, start):
        return add_rows(total, gated, piece, start)

    start_out = jnp.zeros((tok_rows, model_width), jnp.float32)
    result = folded(proj_out, ("sp", "dp"), 0, add_out, start_out)
    return result.astype(jnp.bfloat16).reshape(1, tok_rows, model_width)


def solution(mesh):
    return jax.shard_map(
        body,
        mesh=mesh,
        in_specs=(
            P("dp", "sp", None),
            P(("sp", "dp"), None),
            P(("sp", "dp"), None),
            P(),
            P(None, "dp", None),
            P(),
            P(("sp", "dp"), None),
        ),
        out_specs=P("dp", "sp", None),
        check_vma=False,
    )
```

profile of v0, /device:TPU:0, one launch (start us, length us, event | category | flops | bytes accessed | tf_op | source)
XLA Modules:
  0.0 230.9 jit_solution(3188020381893076137)
XLA Ops:
  6.5 0.0 copy-start
  6.5 0.0 all-gather.8.cloned.1.call-start
  6.5 0.7 all-gather.8.cloned.1.call-update
  7.3 0.0 all-gather.12.cloned.1.call-start
  7.3 2.4 %constant_dynamic-slice_fusion.1 = bf16[1,512,1024]{2,1,0:T(8,128)(2,1)} fusion(bf16[4,512,1024]{2,1,0:T(8,128)(2,1)} %param.11, s32[]{:T(128)S(6)} %select_n.35), kind=kLoop, calls=%fused_computation.29 | loop fusion | bytes 2097156 | tf_op jit(solution)/shard_map/jit(dynamic_index_in_dim)/dynamic_slice | solution.py:42
  9.7 0.0 copy-start.1
  9.7 0.0 all-gather.12.cloned.1.call-update
  9.7 0.0 all-gather.10.cloned.1.call-start
  9.8 0.7 all-gather.10.cloned.1.call-update
  10.4 0.0 all-gather.6.cloned.1.call-start
  10.5 0.5 all-gather.6.cloned.1.call-update
  11.0 58.4 %all-gather.8.cloned.1.call-done = bf16[1024,1024]{1,0:T(8,128)(2,1)} async-done(((bf16[32,1024]{1,0:T(8,128)(2,1)}), bf16[1024,1024]{1,0:T(8,128)(2,1)}) %all-gather.8.cloned.1.call-update) | async-done | bytes 2097168 | tf_op jit(solution)/shard_map/all_gather | solution.py:12
  69.4 0.0 copy-done
  69.4 2.1 fusion.27
  71.5 0.2 multiply_reduce_fusion
  71.8 0.0 copy-done.1
  71.8 0.1 multiply_convert_fusion
  71.9 0.8 copy.13
  72.8 4.5 %all-to-all-start = ((bf16[128,16,64]{0,2,1:T(8,128)(2,1)}), bf16[128,16,64]{0,2,1:T(8,128)(2,1)S(1)}, u32[]{:S(2)}, u32[]{:S(2)}) async-start(bf16[128,16,64]{0,2,1:T(8,128)(2,1)} %bitcast.1), calls=%async_computation | async-start | bytes 524288 | tf_op jit(solution)/shard_map/all_to_all | solution.py:57
  77.3 0.7 constant_dynamic-slice_fusion
  78.0 9.3 %all-to-all-done = bf16[128,16,64]{0,2,1:T(8,128)(2,1)S(1)} async-done(((bf16[128,16,64]{0,2,1:T(8,128)(2,1)}), bf16[128,16,64]{0,2,1:T(8,128)(2,1)S(1)}, u32[]{:S(2)}, u32[]{:S(2)}) %all-to-all-start) | async-done | bytes 262176 | tf_op jit(solution)/shard_map/all_to_all | solution.py:57
  87.3 0.2 copy.14
  87.5 0.1 reshape.110
  87.5 15.4 %all-gather.12.cloned.1.call-done = bf16[1,1024,1024]{2,1,0:T(8,128)(2,1)} async-done(((bf16[1,512,1024]{2,1,0:T(8,128)(2,1)}), bf16[1,1024,1024]{2,1,0:T(8,128)(2,1)}) %all-gather.12.cloned.1.call-update) | async-done | bytes 2097168 | tf_op jit(solution)/shard_map/all_gather | solution.py:43
  103.0 2.5 %fusion.15 = bf16[2,1024,64]{1,2,0:T(8,128)(2,1)S(1)} fusion(bf16[1,1024,1024]{2,1,0:T(8,128)(2,1)} %all-gather.12.cloned.1.call-done, s32[1024]{0:T(1024)S(1)} %add_select_fusion, bf16[2,1024,64]{1,0,2:T(2,128)(2,1)S(1)} %reshape.110, f32[1024]{0:T(1024)S(1)} %bitcast.45), kind=kOutput, calls=%fused_computation.14 | convolution fusion | flops 270794752 | bytes 2629632 | tf_op jit(solution)/shard_map/ij,njc->nic/dot_general | solution.py:53
  105.5 0.3 copy.16
  105.8 0.2 all_to_all.25
  106.0 0.1 copy.17
  106.0 15.9 %all_to_all.29 = bf16[16,128,64]{1,2,0:T(8,128)(2,1)S(1)} all-to-all(bf16[16,128,64]{1,2,0:T(8,128)(2,1)S(1)} %copy.17), channel_id=1, replica_groups=mesh['sp'=16,'dp'=2] {'sp'}, dimensions={0} | all-to-all | bytes 524288 | tf_op jit(solution)/shard_map/all_to_all | solution.py:58
  122.0 0.2 copy.18
  122.2 40.4 %all-gather.10.cloned.1.call-done = bf16[1024,1024]{1,0:T(8,128)(2,1)} async-done(((bf16[32,1024]{1,0:T(8,128)(2,1)}), bf16[1024,1024]{1,0:T(8,128)(2,1)}) %all-gather.10.cloned.1.call-update) | async-done | bytes 2097168 | tf_op jit(solution)/shard_map/all_gather | solution.py:12
  162.6 58.1 %all-gather.6.cloned.1.call-done = bf16[1024,1024]{1,0:T(8,128)(2,1)} async-done(((bf16[32,1024]{1,0:T(8,128)(2,1)}), bf16[1024,1024]{1,0:T(8,128)(2,1)}) %all-gather.6.cloned.1.call-update) | async-done | bytes 2097168 | tf_op jit(solution)/shard_map/all_gather | solution.py:12
  220.7 3.7 %fusion.14 = bf16[1,128,1024]{2,1,0:T(8,128)(2,1)} fusion(bf16[1024,1024]{1,0:T(8,128)(2,1)} %all-gather.10.cloned.1.call-done, f32[128,1024]{1,0:T(8,128)S(1)} %copy.18, bf16[1024,1024]{1,0:T(8,128)(2,1)} %all-gather.6.cloned.1.call-done, bf16[1,128,1024]{2,1,0:T(8,128)(2,1)S(1)} %copy-done), kind=kOutput, calls=%fused_computation.13 | convolution fusion | flops 537526272 | bytes 5242880 | tf_op jit(solution)/shard_map/dot_general | solution.py:19
  (4 shorter events, 0.1 us)
Async XLA Ops:
  6.5 62.9 %copy-start = (bf16[1,128,1024]{2,1,0:T(8,128)(2,1)S(1)}, bf16[1,128,1024]{2,1,0:T(8,128)(2,1)}, u32[]{:S(2)}) copy-start(bf16[1,128,1024]{2,1,0:T(8,128)(2,1)} %param.7) | copy-start | bytes 786436
  6.5 62.9 %all-gather.8.cloned.1.call-start = ((), (), s32[]{:S(2)}) async-start(), calls=%async_computation.3 | async-start | bytes 2162688 | tf_op jit(solution)/shard_map/all_gather | solution.py:12
  7.3 95.7 %all-gather.12.cloned.1.call-start = ((), (), s32[]{:S(2)}) async-start(), calls=%async_computation.5 | async-start | bytes 3145728 | tf_op jit(solution)/shard_map/all_gather | solution.py:43
  9.7 62.1 %copy-start.1 = (f32[1024]{0:T(1024)S(1)}, f32[1024]{0:T(1024)}, u32[]{:S(2)}) copy-start(f32[1024]{0:T(1024)} %param.10) | copy-start | bytes 12292
  9.7 152.9 %all-gather.10.cloned.1.call-start = ((), (), s32[]{:S(2)}) async-start(), calls=%async_computation.4 | async-start | bytes 2162688 | tf_op jit(solution)/shard_map/all_gather | solution.py:12
  10.4 210.3 %all-gather.6.cloned.1.call-start = ((), (), s32[]{:S(2)}) async-start(), calls=%async_computation.2 | async-start | bytes 2162688 | tf_op jit(solution)/shard_map/all_gather | solution.py:12
  72.8 14.5 %all-to-all-start = ((bf16[128,16,64]{0,2,1:T(8,128)(2,1)}), bf16[128,16,64]{0,2,1:T(8,128)(2,1)S(1)}, u32[]{:S(2)}, u32[]{:S(2)}) async-start(bf16[128,16,64]{0,2,1:T(8,128)(2,1)} %bitcast.1), calls=%async_computation | async-start | bytes 524288 | tf_op jit(solution)/shard_map/all_to_all | solution.py:57
Sparse Core Ops, SparseCore 0:
  10.3 59.0 all-gather.7
  71.0 31.9 all-gather.11
  106.0 56.5 all-gather.9
  165.4 55.2 all-gather.5
where the time goes:
time: 231 us
  waiting for transfers between devices  184 us (80%)
  blocking collectives  15.9 us (7%)
  between operations  13.2 us (6%)
  matrix products  8.32 us (4%)
  local copies, waits for them, and re-layouts  4.89 us (2%)
  starting transfers between devices  4.63 us (2%)
    all_gather x3, waiting for transfers between devices, gathered(): return lax.all_gather(part, axis, axis=dim, tiled=True)  157 us
    all_to_all x1, blocking collectives, body(): lax.all_to_all(spatial_mix(sequence), 'sp', split_axis=0, concat_axis=1,...  15.9 us
    all_gather x1, waiting for transfers between devices, body(): head_rows = lax.all_gather(own_rows, 'dp', axis=0, tiled=True)  15.4 us
    all_to_all x1, waiting for transfers between devices, body(): lax.all_to_all(normed, 'sp', split_axis=1, concat_axis=0, tiled=True)  9.27 us
    dot_general x2, matrix products, add_rows(): return total + jnp.dot(columns, piece, preferred_element_type=jnp.float32)  5.79 us
  transfers between devices with their start and end apart: 5, of which 5 were waited for; matrix products, arithmetic and copies ran while one was open for 4% of the time, Pallas kernels for 0%

commit v1 on v0

v1 whole, which is shorter than its diff:
```python
import functools

import jax
import jax.numpy as jnp
from jax import lax
from jax.experimental import pallas as pl
from jax.experimental.pallas import tpu as pltpu
from jax.sharding import PartitionSpec as P

HEAD_DIM = 256
SPAN = 64
EPS = 1e-05
NT = (((1,), (1,)), ((), ()))


def dot_nt(left, right):
    return lax.dot_general(left, right, NT, preferred_element_type=jnp.float32)


def kernel(n_sp, n_dp, tok, wg, wv, gain, mix, bias, wo, out,
           toks, wbuf, mbuf, stats, gat, ubuf, vbuf, osend,
           tok_s, tok_r, w_s, w_r, m_l, m_s, m_r, st_s, st_r, g_s, g_r, o_s, o_r):
    rows, model = tok.shape
    width = gain.shape[1]
    block = mix.shape[2]
    n = block // rows
    chips = n // 2
    cols = width // n
    depth = wg.shape[0]
    mrows = mix.shape[1]
    mhalf = mrows // 2
    total = n_sp * n_dp
    sp, dp = lax.axis_index("sp"), lax.axis_index("dp")
    p = lax.rem(sp, n)
    base = sp - p
    chip, core = lax.div(p, 2), lax.rem(p, 2)
    partner = {"sp": base + chip * 2 + 1 - core, "dp": dp}
    me = sp * n_dp + dp
    head = lax.div(p * cols, HEAD_DIM)

    def copy(src, dst, ssem, rsem, device):
        return pltpu.make_async_remote_copy(
            src_ref=src, dst_ref=dst, send_sem=ssem, recv_sem=rsem,
            device_id=device, device_id_type=pl.DeviceIdType.MESH)

    def device(line):
        return {"sp": lax.div(line, n_dp), "dp": lax.rem(line, n_dp)}

    barrier = pltpu.get_barrier_semaphore()

    @pl.loop(1, total)
    def _(off):
        pl.semaphore_signal(barrier, inc=1, device_id=device(lax.rem(me + off, total)),
                            device_id_type=pl.DeviceIdType.MESH)

    pl.semaphore_wait(barrier, total - 1)

    def slot_of(k, side):
        return lax.rem(chip + chips - k, chips) * 2 + side

    def spread(src, buf, ssem, rsem):
        started = []
        for k in range(1, chips):
            peer = base + lax.rem(chip + k, chips) * 2 + core
            started.append(copy(src, buf.at[p], ssem.at[k], rsem.at[p], {"sp": peer, "dp": dp}))
        started.append(copy(src, buf.at[p], ssem.at[0], rsem.at[p], partner))
        for one in started:
            one.start()
        return started

    def relay(k, buf, ssem, rsem):
        slot = slot_of(k, core)
        one = copy(buf.at[slot], buf.at[slot], ssem.at[chips - 1 + k], rsem.at[slot], partner)
        one.wait_recv()
        one.start()
        return one

    def arrive(k, buf, ssem, rsem):
        slot = slot_of(k, 1 - core)
        copy(buf.at[slot], buf.at[slot], ssem.at[0], rsem.at[slot], partner).wait_recv()

    sent = spread(tok, toks, tok_s, tok_r)

    def weight_sends(i, w):
        @pl.loop(1, total)
        def _(off):
            to = device(lax.rem(me + off, total))
            start = pl.multiple_of(lax.rem(to["sp"], n) * cols, cols)
            copy(w.at[:, pl.ds(start, cols)], wbuf.at[i, me], w_s.at[i], w_r.at[i], to).start()

    weight_sends(1, wv)
    weight_sends(0, wg)
    mine = pltpu.make_async_copy(
        mix.at[head], mbuf.at[pl.ds(pl.multiple_of(dp * mrows, mrows), mrows)], m_l)
    mine.start()
    for k in range(1, n_dp):
        to = lax.rem(dp + k, n_dp)
        span = pl.ds(pl.multiple_of(dp * mrows + core * mhalf, mhalf), mhalf)
        one = copy(mix.at[head, pl.ds(pl.multiple_of(core * mhalf, mhalf), mhalf)], mbuf.at[span],
                   m_s.at[k], m_r.at[dp * 2 + core], {"sp": sp, "dp": to})
        one.start()
        sent.append(one)
    weight_sends(2, wo)

    own = pl.ds(pl.multiple_of(p * cols, cols), cols)
    toks[p] = tok[...]
    for i, w in enumerate((wg, wv, wo)):
        wbuf[i, me] = w[:, own]

    for k in range(1, chips):
        sent.append(relay(k, toks, tok_s, tok_r))

    def weight_wait(sem, i):
        part = wbuf.at[i, pl.ds(0, total - 1)]
        pltpu.make_async_copy(part, part, sem.at[i]).wait()

    def columns_t(i):
        flat = wbuf[i].astype(jnp.float32).reshape(total * depth, cols)
        return jnp.transpose(flat).astype(jnp.bfloat16)

    weight_wait(w_r, 1)
    weight_wait(w_r, 0)
    both = jnp.concatenate([columns_t(0), columns_t(1)], axis=0)
    pair = 2 * rows
    for k in range(chips):
        arrive(k, toks, tok_s, tok_r)
        at = lax.rem(chip + chips - k, chips)
        part = toks[pl.ds(at * 2, 2)].reshape(pair, model)
        result = dot_nt(both, part)
        lanes = pl.ds(pl.multiple_of(at * pair, pair), pair)
        ubuf[:, lanes] = result[:cols].astype(jnp.bfloat16)
        v = result[cols:].astype(jnp.bfloat16).astype(jnp.float32)
        vbuf[:, lanes] = v
        total_v = jnp.sum(v, axis=0, keepdims=True)
        away = v - total_v * (1.0 / cols)
        stats[p, 0:1, lanes] = total_v
        stats[p, 1:2, lanes] = jnp.sum(away * away, axis=0, keepdims=True)

    for k in range(1, n):
        peer = base + lax.rem(p + k, n)
        one = copy(stats.at[p], stats.at[p], st_s.at[k], st_r.at[p], {"sp": peer, "dp": dp})
        one.start()
        sent.append(one)

    mine.wait()
    for k in range(1, n_dp):
        of = lax.rem(dp + n_dp - k, n_dp)
        span = pl.ds(pl.multiple_of(of * mrows + core * mhalf, mhalf), mhalf)
        one = copy(mbuf.at[span], mbuf.at[span], m_s.at[n_dp - 1 + k], m_r.at[of * 2 + core], partner)
        one.wait_recv()
        one.start()
        sent.append(one)
    for k in range(1, n_dp):
        of = lax.rem(dp + n_dp - k, n_dp)
        span = pl.ds(pl.multiple_of(of * mrows + (1 - core) * mhalf, mhalf), mhalf)
        copy(mbuf.at[span], mbuf.at[span], m_s.at[0], m_r.at[of * 2 + 1 - core], partner).wait_recv()

    gain_t = jnp.transpose(jnp.broadcast_to(gain[:, own], (cols, cols)))[:, 0:1]
    for k in range(1, n):
        slot = lax.rem(p + n - k, n)
        copy(stats.at[slot], stats.at[slot], st_s.at[0], st_r.at[slot], partner).wait_recv()
    sums = [stats[q, 0:1, :] for q in range(n)]
    mean = functools.reduce(jnp.add, sums) * (1.0 / width)
    square = jnp.zeros_like(mean)
    for q in range(n):
        gap = sums[q] * (1.0 / cols) - mean
        square = square + stats[q, 1:2, :] + cols * (gap * gap)
    scale = lax.rsqrt(square * (1.0 / width) + EPS)
    normed = ((vbuf[...] - mean) * scale * gain_t).astype(jnp.bfloat16)

    tile = pair
    row = lax.broadcasted_iota(jnp.int32, (tile, tile), 0) // SPAN
    col = lax.broadcasted_iota(jnp.int32, (tile, tile), 1) // SPAN
    bias_row = bias[pl.ds(head, 1), :]
    for t in range(block // tile):
        lo, hi = t * tile, (t + 1) * tile
        diag = mbuf[lo:hi, lo:hi]
        diag = jnp.where(col <= row, diag.astype(jnp.float32), 0.0).astype(jnp.bfloat16)
        mixed = dot_nt(normed[:, lo:hi], diag)
        if t:
            mixed = mixed + dot_nt(normed[:, :lo], mbuf[lo:hi, :lo])
        mixed = (mixed + bias_row[:, lo:hi]).astype(jnp.bfloat16).astype(jnp.float32)
        gat[p, :, lo:hi] = (ubuf[:, lo:hi].astype(jnp.float32) * mixed).astype(jnp.bfloat16)

    sent += spread(gat.at[p], gat, g_s, g_r)
    weight_wait(w_r, 2)
    wo_t = columns_t(2)
    for k in range(1, chips):
        sent.append(relay(k, gat, g_s, g_r))
    for k in range(chips):
        arrive(k, gat, g_s, g_r)

    for k in range(chips):
        at = lax.rem(chip + 1 + k, chips)
        lanes = pl.ds(pl.multiple_of(at * pair, pair), pair)
        right = gat[:, :, lanes].reshape(width, pair)
        result = jnp.dot(wo_t, right, preferred_element_type=jnp.float32)
        turned = jnp.transpose(result).astype(jnp.bfloat16)
        osend[pl.ds(at * 2, 2)] = turned.reshape(2, rows, cols)
        if k < chips - 1:
            for side in range(2):
                one = copy(osend.at[at * 2 + side], out.at[:, own], o_s.at[2 * k + side], o_r.at[p],
                           {"sp": base + at * 2 + side, "dp": dp})
                one.start()
                sent.append(one)
    one = copy(osend.at[chip * 2 + 1 - core], out.at[:, own], o_s.at[n - 1], o_r.at[p], partner)
    one.start()
    sent.append(one)
    out[:, own] = osend[p]
    for k in range(1, n):
        slot = lax.rem(p + n - k, n)
        there = out.at[:, pl.ds(pl.multiple_of(slot * cols, cols), cols)]
        copy(osend.at[0], there, o_s.at[0], o_r.at[slot], partner).wait_recv()
    for one in sent:
        one.wait_send()
    for i in range(3):
        weight_wait(w_s, i)


def body(n_sp, n_dp, tokens, proj_gate, proj_value, norm_gain, mix_weight, mix_bias, proj_out):
    rows, model = tokens.shape[1:]
    width = norm_gain.shape[0]
    block = mix_weight.shape[2]
    n = block // rows
    cols = width // n
    depth = proj_gate.shape[0]
    total = n_sp * n_dp
    vmem = pl.BlockSpec(memory_space=pltpu.VMEM)
    dma = pltpu.SemaphoreType.DMA
    result = pl.pallas_call(
        functools.partial(kernel, n_sp, n_dp),
        out_shape=jax.ShapeDtypeStruct((rows, model), jnp.bfloat16),
        in_specs=[vmem, vmem, vmem, vmem, pl.BlockSpec(memory_space=pl.ANY), vmem, vmem],
        out_specs=vmem,
        scratch_shapes=[
            pltpu.VMEM((n, rows, model), jnp.bfloat16),
            pltpu.VMEM((3, total, depth, cols), jnp.bfloat16),
            pltpu.VMEM((block, block), jnp.bfloat16),
            pltpu.VMEM((n, 2, block), jnp.float32),
            pltpu.VMEM((n, cols, block), jnp.bfloat16),
            pltpu.VMEM((cols, block), jnp.bfloat16),
            pltpu.VMEM((cols, block), jnp.float32),
            pltpu.VMEM((n, rows, cols), jnp.bfloat16),
            dma((n,)), dma((n,)), dma((3,)), dma((3,)),
            dma, dma((2 * n_dp,)), dma((2 * n_dp,)),
            dma((n,)), dma((n,)), dma((n,)), dma((n,)), dma((n,)), dma((n,)),
        ],
        compiler_params=pltpu.CompilerParams(
            collective_id=0, has_side_effects=True, vmem_limit_bytes=32 * 1024 * 1024),
    )(tokens.reshape(rows, model), proj_gate, proj_value, norm_gain.reshape(1, width),
      mix_weight, mix_bias, proj_out)
    return result.reshape(1, rows, model)


def solution(mesh):
    return jax.shard_map(
        functools.partial(body, mesh.shape["sp"], mesh.shape["dp"]),
        mesh=mesh,
        in_specs=(
            P("dp", "sp", None),
            P(("sp", "dp"), None),
            P(("sp", "dp"), None),
            P(),
            P(None, "dp", None),
            P(),
            P(("sp", "dp"), None),
        ),
        out_specs=P("dp", "sp", None),
        check_vma=False,
    )
```

time: 231 us -> 66.2 us (0.29)
  waiting for transfers between devices: 184 us -> 0 us
  Pallas kernels: 0 us -> 58.1 us
  blocking collectives: 15.9 us -> 0 us
  between operations: 13.2 us -> 0.02 us
  matrix products: 8.32 us -> 0 us
  starting transfers between devices: 4.63 us -> 0 us
  local copies, waits for them, and re-layouts: 4.89 us -> 7.76 us
    all_gather x4 -> x0, waiting for transfers between devices: 172 us -> none  [the longest x3 157 us: gathered(): return lax.all_gather(part, axis, axis=dim, tiled=True)]
    pallas_call x0 -> x1, Pallas kernels: none -> 58.1 us  [body(): pl.pallas_call(functools.partial(kernel, n_sp, n_dp), out_shape=jax.Shape...]
    all_to_all x1 -> x0, blocking collectives: 15.9 us -> none  [body(): lax.all_to_all(spatial_mix(sequence), 'sp', split_axis=0, concat_axis=1,...]
    all_to_all x1 -> x0, waiting for transfers between devices: 9.27 us -> none  [body(): lax.all_to_all(normed, 'sp', split_axis=1, concat_axis=0, tiled=True)]
    dot_general x3 -> x0, matrix products: 8.32 us -> none  [the longest x2 5.79 us: add_rows(): return total + jnp.dot(columns, piece, preferred_element_type=jnp.float32)]
    unnamed x4 -> x15, local copies, waits for them, and re-layouts: 0.01 us -> 7.76 us
    all_to_all x1 -> x0, starting transfers between devices: 4.51 us -> none  [body(): lax.all_to_all(normed, 'sp', split_axis=1, concat_axis=0, tiled=True)]
    dynamic_slice x2 -> x0, local copies, waits for them, and re-layouts: 3.09 us -> none  [the longest x1 2.36 us: body(): own_rows = lax.dynamic_index_in_dim(mix_weight, head, 0, keepdims=False)]
  transfers between devices with their start and end apart: 5 -> 0, of which waited for: 5 -> 0; matrix products, arithmetic and copies ran while one was open for 4% -> 0% of each run, Pallas kernels for 0% -> 0%
where the time goes in v1:
time: 66.2 us; the launch traced here: 65.8 us
  Pallas kernels  58.1 us (88%)
  local copies, waits for them, and re-layouts  7.76 us (12%)
    pallas_call x1, Pallas kernels, body(): pl.pallas_call(functools.partial(kernel, n_sp, n_dp), out_shape=jax.Shape...  58.1 us
    unnamed x15, local copies, waits for them, and re-layouts  7.76 us

profile of v1, /device:TPU:0, one launch (start us, length us, event | category | flops | bytes accessed | tf_op | source)
XLA Modules:
  0.0 65.8 jit_solution(2066461079705386279)
XLA Ops:
  0.0 0.0 copy-start
  0.0 2.2 %copy-done = bf16[4,512,1024]{2,1,0:T(8,128)(2,1)S(1)} copy-done((bf16[4,512,1024]{2,1,0:T(8,128)(2,1)S(1)}, bf16[4,512,1024]{2,1,0:T(8,128)(2,1)}, u32[]{:S(2)}) %copy-start) | copy-done | bytes 4194328
  2.2 0.0 copy-start.1
  2.2 0.9 %copy-done.1 = bf16[1,128,1024]{2,1,0:T(8,128)(2,1)S(1)} copy-done((bf16[1,128,1024]{2,1,0:T(8,128)(2,1)S(1)}, bf16[1,128,1024]{2,1,0:T(8,128)(2,1)}, u32[]{:S(2)}) %copy-start.1) | copy-done | bytes 262168
  3.1 0.0 copy-start.2
  3.1 0.8 %copy-done.2 = bf16[32,1024]{1,0:T(8,128)(2,1)S(1)} copy-done((bf16[32,1024]{1,0:T(8,128)(2,1)S(1)}, bf16[32,1024]{1,0:T(8,128)(2,1)}, u32[]{:S(2)}) %copy-start.2) | copy-done | bytes 65560
  4.0 0.0 copy-start.3
  4.0 0.8 %copy-done.3 = bf16[32,1024]{1,0:T(8,128)(2,1)S(1)} copy-done((bf16[32,1024]{1,0:T(8,128)(2,1)S(1)}, bf16[32,1024]{1,0:T(8,128)(2,1)}, u32[]{:S(2)}) %copy-start.3) | copy-done | bytes 65560
  4.8 0.0 copy-start.4
  4.8 0.8 %copy-done.4 = bf16[32,1024]{1,0:T(8,128)(2,1)S(1)} copy-done((bf16[32,1024]{1,0:T(8,128)(2,1)S(1)}, bf16[32,1024]{1,0:T(8,128)(2,1)}, u32[]{:S(2)}) %copy-start.4) | copy-done | bytes 65560
  5.7 0.0 copy-start.5
  5.7 0.7 %copy-done.5 = f32[4,1024]{1,0:T(4,128)S(1)} copy-done((f32[4,1024]{1,0:T(4,128)S(1)}, f32[4,1024]{1,0:T(4,128)}, u32[]{:S(2)}) %copy-start.5) | copy-done | bytes 16408
  6.4 0.0 copy-start.6
  6.4 0.7 %copy-done.6 = f32[1024]{0:T(1024)S(1)} copy-done((f32[1024]{0:T(1024)S(1)}, f32[1024]{0:T(1024)}, u32[]{:S(2)}) %copy-start.6) | copy-done | bytes 4120
  7.1 58.1 %shard_map.73 = bf16[128,1024]{1,0:T(8,128)(2,1)S(1)} custom-call(bf16[128,1024]{1,0:T(8,128)(2,1)S(1)} %bitcast.4, bf16[32,1024]{1,0:T(8,128)(2,1)S(1)} %copy-done.2, bf16[32,1024]{1,0:T(8,128)(2,1)S(1)} %copy-done.3, f32[1,1024]{1,0:T(1,128)S(1)} %bitcast.5, bf16[4,512,1024]{2,1,0:T(8,128)(2,1)S(1)} %copy-done, f32[4,1024]{1,0:T(4,128)S(1)} %copy-done.5, ...), custom_call_target="tpu_custom_call" | custom-call | tf_op jit(solution)/shard_map/pallas_call | solution.py:230
  65.1 0.7 %copy.9 = bf16[1,128,1024]{2,1,0:T(8,128)(2,1)} copy(bf16[1,128,1024]{2,1,0:T(8,128)(2,1)S(1)} %bitcast.3) | data formatting | bytes 524288
Async XLA Ops:
  0.0 2.2 %copy-start = (bf16[4,512,1024]{2,1,0:T(8,128)(2,1)S(1)}, bf16[4,512,1024]{2,1,0:T(8,128)(2,1)}, u32[]{:S(2)}) copy-start(bf16[4,512,1024]{2,1,0:T(8,128)(2,1)} %mix.1) | copy-start | bytes 12582916
  2.2 0.9 %copy-start.1 = (bf16[1,128,1024]{2,1,0:T(8,128)(2,1)S(1)}, bf16[1,128,1024]{2,1,0:T(8,128)(2,1)}, u32[]{:S(2)}) copy-start(bf16[1,128,1024]{2,1,0:T(8,128)(2,1)} %param.7) | copy-start | bytes 786436
  3.1 0.8 %copy-start.2 = (bf16[32,1024]{1,0:T(8,128)(2,1)S(1)}, bf16[32,1024]{1,0:T(8,128)(2,1)}, u32[]{:S(2)}) copy-start(bf16[32,1024]{1,0:T(8,128)(2,1)} %wg.1) | copy-start | bytes 196612
  4.0 0.8 %copy-start.3 = (bf16[32,1024]{1,0:T(8,128)(2,1)S(1)}, bf16[32,1024]{1,0:T(8,128)(2,1)}, u32[]{:S(2)}) copy-start(bf16[32,1024]{1,0:T(8,128)(2,1)} %wv.1) | copy-start | bytes 196612
  4.8 0.8 %copy-start.4 = (bf16[32,1024]{1,0:T(8,128)(2,1)S(1)}, bf16[32,1024]{1,0:T(8,128)(2,1)}, u32[]{:S(2)}) copy-start(bf16[32,1024]{1,0:T(8,128)(2,1)} %wo.1) | copy-start | bytes 196612
  5.7 0.7 %copy-start.5 = (f32[4,1024]{1,0:T(4,128)S(1)}, f32[4,1024]{1,0:T(4,128)}, u32[]{:S(2)}) copy-start(f32[4,1024]{1,0:T(4,128)} %bias.1) | copy-start | bytes 49156
  6.4 0.7 %copy-start.6 = (f32[1024]{0:T(1024)S(1)}, f32[1024]{0:T(1024)}, u32[]{:S(2)}) copy-start(f32[1024]{0:T(1024)} %param.10) | copy-start | bytes 12292

commit v2 on v1

v2 whole, which is shorter than its diff:
```python
import functools

import jax
import jax.numpy as jnp
from jax import lax
from jax.experimental import pallas as pl
from jax.experimental.pallas import tpu as pltpu
from jax.sharding import PartitionSpec as P

HEAD_DIM = 256
SPAN = 64
EPS = 1e-05
NT = (((1,), (1,)), ((), ()))


def dot_nt(left, right):
    return lax.dot_general(left, right, NT, preferred_element_type=jnp.float32)


def kernel(n_sp, n_dp, tok, wg, wv, gain_in, mix, bias_in, wo, out,
           toks, wloc, wbuf, mbuf, dbuf, gain, bias, stats, gat, ubuf, vbuf, osend,
           l_s, tok_s, tok_r, w_s, w_r, x_s, x_r, m_s, m_r, st_s, st_r, g_s, g_r, o_s, o_r):
    rows, model = tok.shape
    width = gain.shape[1]
    block = mix.shape[2]
    n = block // rows
    chips = n // 2
    cols = width // n
    depth = wg.shape[0]
    mrows = mix.shape[1]
    mhalf = mrows // 2
    pair = 2 * rows
    sp, dp = lax.axis_index("sp"), lax.axis_index("dp")
    p = lax.rem(sp, n)
    base = sp - p
    chip, core = lax.div(p, 2), lax.rem(p, 2)
    partner = {"sp": base + chip * 2 + 1 - core, "dp": dp}
    head = lax.div(p * cols, HEAD_DIM)
    own = pl.ds(pl.multiple_of(p * cols, cols), cols)
    mine = pl.ds(pl.multiple_of(dp * mrows, mrows), mrows)

    def copy(src, dst, ssem, rsem, device):
        return pltpu.make_async_remote_copy(
            src_ref=src, dst_ref=dst, send_sem=ssem, recv_sem=rsem,
            device_id=device, device_id_type=pl.DeviceIdType.MESH)

    def at_sp(index):
        return {"sp": index, "dp": dp}

    loads = [(wg, wloc.at[0]), (wv, wloc.at[1]), (wo, wloc.at[2]), (tok, toks.at[p]),
             (gain_in, gain), (bias_in, bias), (mix.at[head], mbuf.at[mine])]
    loads += [(w.at[:, own], wbuf.at[i, sp, dp]) for i, w in enumerate((wg, wv, wo))]
    loads = [pltpu.make_async_copy(src, dst, l_s.at[i]) for i, (src, dst) in enumerate(loads)]
    for one in loads:
        one.start()

    barrier = pltpu.get_barrier_semaphore()

    @pl.loop(1, n_sp)
    def _(off):
        pl.semaphore_signal(barrier, inc=1, device_id=at_sp(lax.rem(sp + off, n_sp)),
                            device_id_type=pl.DeviceIdType.MESH)

    for k in range(1, n_dp):
        pl.semaphore_signal(barrier, inc=1, device_id={"sp": sp, "dp": lax.rem(dp + k, n_dp)},
                            device_id_type=pl.DeviceIdType.MESH)
    pl.semaphore_wait(barrier, n_sp + n_dp - 2)
    for one in loads:
        one.wait()
    sent = []

    def start(one):
        one.start()
        sent.append(one)

    def slot_of(k, side):
        return lax.rem(chip + chips - k, chips) * 2 + side

    def spread(view, ssem, rsem):
        for k in range(1, chips):
            peer = base + lax.rem(chip + k, chips) * 2 + core
            start(copy(view(p), view(p), ssem(k), rsem(p), at_sp(peer)))
        start(copy(view(p), view(p), ssem(0), rsem(p), partner))

    def relay(k, view, ssem, rsem):
        slot = slot_of(k, core)
        one = copy(view(slot), view(slot), ssem(chips - 1 + k), rsem(slot), partner)
        one.wait_recv()
        start(one)

    def arrive(k, view, ssem, rsem):
        slot = slot_of(k, 1 - core)
        copy(view(slot), view(slot), ssem(0), rsem(slot), partner).wait_recv()

    def weight_sends(i):
        @pl.loop(1, n_sp)
        def _(off):
            to = lax.rem(sp + off, n_sp)
            lanes = pl.ds(pl.multiple_of(lax.rem(to, n) * cols, cols), cols)
            copy(wloc.at[i, :, lanes], wbuf.at[i, sp, dp], w_s.at[i], w_r.at[i], at_sp(to)).start()

    def weight_wait(sem, i):
        part = wbuf.at[i, pl.ds(0, n_sp - 1), 0]
        pltpu.make_async_copy(part, part, sem.at[i]).wait()

    def weight_relay(i):
        weight_wait(w_r, i)
        part = wbuf.at[i, :, dp]
        for k in range(1, n_dp):
            start(copy(part, part, x_s.at[i, k], x_r.at[i, dp], {"sp": sp, "dp": lax.rem(dp + k, n_dp)}))

    def columns_t(i):
        for k in range(1, n_dp):
            of = lax.rem(dp + n_dp - k, n_dp)
            part = wbuf.at[i, :, of]
            copy(part, part, x_s.at[i, 0], x_r.at[i, of], partner).wait_recv()
        flat = wbuf[i].astype(jnp.float32).reshape(n_sp * n_dp * depth, cols)
        return jnp.transpose(flat).astype(jnp.bfloat16)

    tok_view = (lambda q: toks.at[q], lambda k: tok_s.at[k], lambda q: tok_r.at[q])

    def gat_view(t):
        lanes = pl.ds(t * pair, pair)
        return (lambda q: gat.at[q, :, lanes], lambda k: g_s.at[t, k], lambda q: g_r.at[t, q])

    weight_sends(1)
    weight_sends(0)
    spread(*tok_view)
    weight_sends(2)
    weight_relay(1)
    weight_relay(0)
    for k in range(1, n_dp):
        span = pl.ds(pl.multiple_of(dp * mrows + core * mhalf, mhalf), mhalf)
        start(copy(mbuf.at[span], mbuf.at[span], m_s.at[k], m_r.at[dp * 2 + core],
                   {"sp": sp, "dp": lax.rem(dp + k, n_dp)}))

    both = jnp.concatenate([columns_t(0), columns_t(1)], axis=0)
    for k in range(chips):
        if k + 1 < chips:
            relay(k + 1, *tok_view)
        arrive(k, *tok_view)
        at = lax.rem(chip + chips - k, chips)
        part = toks[pl.ds(at * 2, 2)].reshape(pair, model)
        result = dot_nt(both, part)
        lanes = pl.ds(pl.multiple_of(at * pair, pair), pair)
        ubuf[:, lanes] = result[:cols].astype(jnp.bfloat16)
        v = result[cols:].astype(jnp.bfloat16).astype(jnp.float32)
        vbuf[:, lanes] = v
        total_v = jnp.sum(v, axis=0, keepdims=True)
        away = v - total_v * (1.0 / cols)
        stats[p, 0:1, lanes] = total_v
        stats[p, 1:2, lanes] = jnp.sum(away * away, axis=0, keepdims=True)

    for k in range(1, n):
        start(copy(stats.at[p], stats.at[p], st_s.at[k], st_r.at[p], at_sp(base + lax.rem(p + k, n))))

    for k in range(1, n_dp):
        of = lax.rem(dp + n_dp - k, n_dp)
        span = pl.ds(pl.multiple_of(of * mrows + core * mhalf, mhalf), mhalf)
        one = copy(mbuf.at[span], mbuf.at[span], m_s.at[n_dp - 1 + k], m_r.at[of * 2 + core], partner)
        one.wait_recv()
        start(one)
    weight_relay(2)
    for k in range(1, n_dp):
        of = lax.rem(dp + n_dp - k, n_dp)
        span = pl.ds(pl.multiple_of(of * mrows + (1 - core) * mhalf, mhalf), mhalf)
        copy(mbuf.at[span], mbuf.at[span], m_s.at[0], m_r.at[of * 2 + 1 - core], partner).wait_recv()

    row = lax.broadcasted_iota(jnp.int32, (pair, pair), 0) // SPAN
    col = lax.broadcasted_iota(jnp.int32, (pair, pair), 1) // SPAN
    for t in range(chips):
        lo, hi = t * pair, (t + 1) * pair
        diag = mbuf[lo:hi, lo:hi].astype(jnp.float32)
        dbuf[t] = jnp.where(col <= row, diag, 0.0).astype(jnp.bfloat16)
    gain_t = jnp.transpose(jnp.broadcast_to(gain[:, own], (cols, cols)))[:, 0:1]
    for k in range(1, n):
        slot = lax.rem(p + n - k, n)
        copy(stats.at[slot], stats.at[slot], st_s.at[0], st_r.at[slot], partner).wait_recv()
    sums = [stats[q, 0:1, :] for q in range(n)]
    mean = functools.reduce(jnp.add, sums) * (1.0 / width)
    square = jnp.zeros_like(mean)
    for q in range(n):
        gap = sums[q] * (1.0 / cols) - mean
        square = square + stats[q, 1:2, :] + cols * (gap * gap)
    scale = lax.rsqrt(square * (1.0 / width) + EPS)
    normed = ((vbuf[...] - mean) * scale * gain_t).astype(jnp.bfloat16)

    bias_row = bias[pl.ds(head, 1), :]
    for t in range(chips):
        lo, hi = t * pair, (t + 1) * pair
        mixed = dot_nt(normed[:, lo:hi], dbuf[t])
        if t:
            mixed = mixed + dot_nt(normed[:, :lo], mbuf[lo:hi, :lo])
        mixed = (mixed + bias_row[:, lo:hi]).astype(jnp.bfloat16).astype(jnp.float32)
        gat[p, :, lo:hi] = (ubuf[:, lo:hi].astype(jnp.float32) * mixed).astype(jnp.bfloat16)
        spread(*gat_view(t))

    wo_t = columns_t(2)
    for t in range(chips):
        for k in range(1, chips):
            relay(k, *gat_view(t))
        for k in range(chips):
            arrive(k, *gat_view(t))
        right = gat[:, :, t * pair:(t + 1) * pair].reshape(width, pair)
        result = jnp.dot(wo_t, right, preferred_element_type=jnp.float32)
        turned = jnp.transpose(result).astype(jnp.bfloat16)
        osend[2 * t:2 * t + 2] = turned.reshape(2, rows, cols)
        for q in (2 * t, 2 * t + 1):
            @pl.when(p != q)
            def _():
                copy(osend.at[q], out.at[:, own], o_s.at[q], o_r.at[p], at_sp(base + q)).start()

            @pl.when(p == q)
            def _():
                out[:, own] = osend[q]

    for k in range(1, n):
        slot = lax.rem(p + n - k, n)
        there = out.at[:, pl.ds(pl.multiple_of(slot * cols, cols), cols)]
        copy(osend.at[0], there, o_s.at[0], o_r.at[slot], partner).wait_recv()
    for k in range(1, n):
        q = lax.rem(p + k, n)
        copy(osend.at[q], out.at[:, own], o_s.at[q], o_r.at[p], at_sp(base + q)).wait_send()
    for one in sent:
        one.wait_send()
    for i in range(3):
        weight_wait(w_s, i)


def body(n_sp, n_dp, tokens, proj_gate, proj_value, norm_gain, mix_weight, mix_bias, proj_out):
    rows, model = tokens.shape[1:]
    width = norm_gain.shape[0]
    block = mix_weight.shape[2]
    n = block // rows
    cols = width // n
    depth = proj_gate.shape[0]
    chips = n // 2
    hbm = pl.BlockSpec(memory_space=pltpu.HBM)
    dma = pltpu.SemaphoreType.DMA
    result = pl.pallas_call(
        functools.partial(kernel, n_sp, n_dp),
        out_shape=jax.ShapeDtypeStruct((rows, model), jnp.bfloat16),
        in_specs=[hbm] * 7,
        out_specs=pl.BlockSpec(memory_space=pltpu.VMEM),
        scratch_shapes=[
            pltpu.VMEM((n, rows, model), jnp.bfloat16),
            pltpu.VMEM((3, depth, width), jnp.bfloat16),
            pltpu.VMEM((3, n_sp, n_dp, depth, cols), jnp.bfloat16),
            pltpu.VMEM((block, block), jnp.bfloat16),
            pltpu.VMEM((chips, 2 * rows, 2 * rows), jnp.bfloat16),
            pltpu.VMEM((1, width), jnp.float32),
            pltpu.VMEM(mix_bias.shape, jnp.float32),
            pltpu.VMEM((n, 2, block), jnp.float32),
            pltpu.VMEM((n, cols, block), jnp.bfloat16),
            pltpu.VMEM((cols, block), jnp.bfloat16),
            pltpu.VMEM((cols, block), jnp.float32),
            pltpu.VMEM((n, rows, cols), jnp.bfloat16),
            dma((10,)), dma((n,)), dma((n,)), dma((3,)), dma((3,)),
            dma((3, n_dp)), dma((3, n_dp)), dma((2 * n_dp,)), dma((2 * n_dp,)),
            dma((n,)), dma((n,)), dma((chips, n)), dma((chips, n)), dma((n,)), dma((n,)),
        ],
        compiler_params=pltpu.CompilerParams(
            collective_id=0, has_side_effects=True, vmem_limit_bytes=60 * 1024 * 1024),
    )(tokens.reshape(rows, model), proj_gate, proj_value, norm_gain.reshape(1, width),
      mix_weight, mix_bias, proj_out)
    return result.reshape(1, rows, model)


def solution(mesh):
    return jax.shard_map(
        functools.partial(body, mesh.shape["sp"], mesh.shape["dp"]),
        mesh=mesh,
        in_specs=(
            P("dp", "sp", None),
            P(("sp", "dp"), None),
            P(("sp", "dp"), None),
            P(),
            P(None, "dp", None),
            P(),
            P(("sp", "dp"), None),
        ),
        out_specs=P("dp", "sp", None),
        check_vma=False,
    )
```

time: 66.2 us -> 54 us (0.82)
  Pallas kernels: 58.1 us -> 51.8 us
  local copies, waits for them, and re-layouts: 7.76 us -> 1.67 us
    pallas_call x1, Pallas kernels: 58.1 us -> 51.8 us  [body(): pl.pallas_call(functools.partial(kernel, n_sp, n_dp), out_shape=jax.Shape...]
    unnamed x15 -> x1, local copies, waits for them, and re-layouts: 7.76 us -> 1.67 us
where the time goes in v2:
time: 54 us; the launch traced here: 53.5 us
  Pallas kernels  51.8 us (96%)
  local copies, waits for them, and re-layouts  1.67 us (3%)
    pallas_call x1, Pallas kernels, body(): pl.pallas_call(functools.partial(kernel, n_sp, n_dp), out_shape=jax.Shape...  51.8 us
    unnamed x1, local copies, waits for them, and re-layouts  1.67 us

profile of v2, /device:TPU:0, one launch (start us, length us, event | category | flops | bytes accessed | tf_op | source)
XLA Modules:
  0.0 53.5 jit_solution(5667069729819450350)
XLA Ops:
  0.0 51.8 %shard_map.73 = bf16[128,1024]{1,0:T(8,128)(2,1)} custom-call(bf16[128,1024]{1,0:T(8,128)(2,1)} %bitcast.4, bf16[32,1024]{1,0:T(8,128)(2,1)} %wg.1, bf16[32,1024]{1,0:T(8,128)(2,1)} %wv.1, f32[1,1024]{1,0:T(1,128)} %bitcast.5, bf16[4,512,1024]{2,1,0:T(8,128)(2,1)} %mix.1, f32[4,1024]{1,0:T(4,128)} %bias_in.1, bf16[32,1024]{1,0:T(8,128)(2,1)} %wo.1), custom_call_target="tpu_custom_call" | custom-call | tf_op jit(solution)/shard_map/pallas_call | solution.py:240
  51.8 1.7 %copy.9 = bf16[1,128,1024]{2,1,0:T(8,128)(2,1)} copy(bf16[1,128,1024]{2,1,0:T(8,128)(2,1)} %bitcast.3) | data formatting | bytes 524288

commit v3 on v2

--- a/solution.py
+++ b/solution.py
@@ -123,16 +123,40 @@
         lanes = pl.ds(t * pair, pair)
         return (lambda q: gat.at[q, :, lanes], lambda k: g_s.at[t, k], lambda q: g_r.at[t, q])
 
+    quarter = mhalf // 2
+
+    def mix_span(of, side, piece):
+        return pl.ds(pl.multiple_of(of * mrows + side * mhalf + piece * quarter, quarter), quarter)
+
+    def mix_send(piece):
+        span = mix_span(dp, core, piece)
+        for k in range(1, n_dp):
+            start(copy(mbuf.at[span], mbuf.at[span], m_s.at[piece, k], m_r.at[piece, dp * 2 + core],
+                       {"sp": sp, "dp": lax.rem(dp + k, n_dp)}))
+
+    def mix_relay(piece):
+        for k in range(1, n_dp):
+            of = lax.rem(dp + n_dp - k, n_dp)
+            span = mix_span(of, core, piece)
+            one = copy(mbuf.at[span], mbuf.at[span], m_s.at[piece, n_dp - 1 + k],
+                       m_r.at[piece, of * 2 + core], partner)
+            one.wait_recv()
+            start(one)
+
+    def mix_arrive(piece):
+        for k in range(1, n_dp):
+            of = lax.rem(dp + n_dp - k, n_dp)
+            span = mix_span(of, 1 - core, piece)
+            copy(mbuf.at[span], mbuf.at[span], m_s.at[piece, 0],
+                 m_r.at[piece, of * 2 + 1 - core], partner).wait_recv()
+
+    mix_send(0)
     weight_sends(1)
     weight_sends(0)
     spread(*tok_view)
-    weight_sends(2)
     weight_relay(1)
     weight_relay(0)
-    for k in range(1, n_dp):
-        span = pl.ds(pl.multiple_of(dp * mrows + core * mhalf, mhalf), mhalf)
-        start(copy(mbuf.at[span], mbuf.at[span], m_s.at[k], m_r.at[dp * 2 + core],
-                   {"sp": sp, "dp": lax.rem(dp + k, n_dp)}))
+    mix_send(1)
 
     both = jnp.concatenate([columns_t(0), columns_t(1)], axis=0)
     for k in range(chips):
@@ -154,17 +178,11 @@
     for k in range(1, n):
         start(copy(stats.at[p], stats.at[p], st_s.at[k], st_r.at[p], at_sp(base + lax.rem(p + k, n))))
 
-    for k in range(1, n_dp):
-        of = lax.rem(dp + n_dp - k, n_dp)
-        span = pl.ds(pl.multiple_of(of * mrows + core * mhalf, mhalf), mhalf)
-        one = copy(mbuf.at[span], mbuf.at[span], m_s.at[n_dp - 1 + k], m_r.at[of * 2 + core], partner)
-        one.wait_recv()
-        start(one)
-    weight_relay(2)
-    for k in range(1, n_dp):
-        of = lax.rem(dp + n_dp - k, n_dp)
-        span = pl.ds(pl.multiple_of(of * mrows + (1 - core) * mhalf, mhalf), mhalf)
-        copy(mbuf.at[span], mbuf.at[span], m_s.at[0], m_r.at[of * 2 + 1 - core], partner).wait_recv()
+    weight_sends(2)
+    for piece in range(2):
+        mix_relay(piece)
+    for piece in range(2):
+        mix_arrive(piece)
 
     row = lax.broadcasted_iota(jnp.int32, (pair, pair), 0) // SPAN
     col = lax.broadcasted_iota(jnp.int32, (pair, pair), 1) // SPAN
@@ -194,6 +212,8 @@
         mixed = (mixed + bias_row[:, lo:hi]).astype(jnp.bfloat16).astype(jnp.float32)
         gat[p, :, lo:hi] = (ubuf[:, lo:hi].astype(jnp.float32) * mixed).astype(jnp.bfloat16)
         spread(*gat_view(t))
+        if t == 1:
+            weight_relay(2)
 
     wo_t = columns_t(2)
     for t in range(chips):
@@ -256,7 +276,7 @@
             pltpu.VMEM((cols, block), jnp.float32),
             pltpu.VMEM((n, rows, cols), jnp.bfloat16),
             dma((10,)), dma((n,)), dma((n,)), dma((3,)), dma((3,)),
-            dma((3, n_dp)), dma((3, n_dp)), dma((2 * n_dp,)), dma((2 * n_dp,)),
+            dma((3, n_dp)), dma((3, n_dp)), dma((2, 2 * n_dp)), dma((2, 2 * n_dp)),
             dma((n,)), dma((n,)), dma((chips, n)), dma((chips, n)), dma((n,)), dma((n,)),
         ],
         compiler_params=pltpu.CompilerParams(

time: 54 us -> 50.7 us (0.939)
  Pallas kernels: 51.8 us -> 48.9 us
    pallas_call x1, Pallas kernels: 51.8 us -> 48.9 us  [body(): pl.pallas_call(functools.partial(kernel, n_sp, n_dp), out_shape=jax.Shape...]
where the time goes in v3:
time: 50.7 us; the launch traced here: 50.5 us
  Pallas kernels  48.9 us (96%)
  local copies, waits for them, and re-layouts  1.67 us (3%)
    pallas_call x1, Pallas kernels, body(): pl.pallas_call(functools.partial(kernel, n_sp, n_dp), out_shape=jax.Shape...  48.9 us
    unnamed x1, local copies, waits for them, and re-layouts  1.67 us

profile of v3, /device:TPU:0, one launch (start us, length us, event | category | flops | bytes accessed | tf_op | source)
XLA Modules:
  0.0 50.5 jit_solution(11736634793062475196)
XLA Ops:
  0.0 48.9 %shard_map.73 = bf16[128,1024]{1,0:T(8,128)(2,1)} custom-call(bf16[128,1024]{1,0:T(8,128)(2,1)} %bitcast.4, bf16[32,1024]{1,0:T(8,128)(2,1)} %wg.1, bf16[32,1024]{1,0:T(8,128)(2,1)} %wv.1, f32[1,1024]{1,0:T(1,128)} %bitcast.5, bf16[4,512,1024]{2,1,0:T(8,128)(2,1)} %mix.1, f32[4,1024]{1,0:T(4,128)} %bias_in.1, bf16[32,1024]{1,0:T(8,128)(2,1)} %wo.1), custom_call_target="tpu_custom_call" | custom-call | tf_op jit(solution)/shard_map/pallas_call | solution.py:260
  48.9 1.7 %copy.9 = bf16[1,128,1024]{2,1,0:T(8,128)(2,1)} copy(bf16[1,128,1024]{2,1,0:T(8,128)(2,1)} %bitcast.3) | data formatting | bytes 524288
